TPU v7x, 32 devices: a whole 2x2x4 slice. The times are simulated.
32 devices in a mesh: fs: 4 (over y, x), tp: 8 (over z, core).
Axes of the slice: x: 2, y: 2, z: 4, core: 2. Of those that a mesh axis runs over, the one named last changes fastest.
Arguments:
- inputs: bfloat16 [1536, 2048], P('fs'), may hold values from -6 to 6
- pre_act: bfloat16 [1536, 8192], P('fs', 'tp'), may hold values from -6 to 6
- cotangent: bfloat16 [1536, 2048], P('fs'), may hold values from -6 to 6
- up_weight: bfloat16 [2048, 8192], P('fs', 'tp'), may hold values from -0.125 to 0.125
- down_weight: bfloat16 [8192, 2048], P('tp', 'fs'), may hold values from -0.0625 to 0.0625
Outputs:
- input_grad: bfloat16 [1536, 2048], P('fs')
- up_grad: float32 [2048, 8192], P('fs', 'tp')
- down_grad: float32 [8192, 2048], P('tp', 'fs')
- up_norms: float32 [2048], P('fs')
- down_norms: float32 [8192], P('tp')
All inputs are finite; a program needn't handle non-finite values.
Results may differ from a plain program's by a relative error of at most 0.0051.
Values may be sent and summed in bfloat16 or wider, within the bound.
A program may use at most 64 MiB of HBM per device.

v0:
```python
import jax
import jax.numpy as jnp
from jax import lax
from jax.sharding import PartitionSpec as P


def contract_last(left, right):
    return lax.dot_general(
        left, right, (((1,), (1,)), ((), ())), preferred_element_type=jnp.float32
    )


def contract_first(left, right):
    return lax.dot_general(
        left, right, (((0,), (0,)), ((), ())), preferred_element_type=jnp.float32
    )


def local(inputs, pre_act, cotangent, up_weight, down_weight):
    active = jnp.maximum(pre_act.astype(jnp.float32), 0.0)
    squared = (active * active).astype(jnp.bfloat16)
    sq_grad = contract_last(cotangent, lax.all_gather(down_weight, "fs", axis=1, tiled=True))
    pre_grad = (2.0 * active * sq_grad).astype(jnp.bfloat16)
    partial_value = contract_last(pre_grad, lax.all_gather(up_weight, "fs", axis=0, tiled=True))
    input_grad = lax.psum(partial_value, "tp").astype(jnp.bfloat16)
    input_cols, cotan_cols = (
        lax.all_to_all(inputs, "fs", split_axis=1, concat_axis=0, tiled=True),
        lax.all_to_all(cotangent, "fs", split_axis=1, concat_axis=0, tiled=True),
    )
    all_pre_grad, all_squared = (
        lax.all_gather(pre_grad, "fs", axis=0, tiled=True),
        lax.all_gather(squared, "fs", axis=0, tiled=True),
    )
    up_grad = contract_first(input_cols, all_pre_grad)
    down_grad = contract_first(all_squared, cotan_cols)
    up_norms = lax.psum(jnp.sum(up_grad * up_grad, axis=1), "tp")
    down_norms = lax.psum(jnp.sum(down_grad * down_grad, axis=1), "fs")
    return (input_grad, up_grad, down_grad, up_norms, down_norms)


def solution(mesh):
    in_specs = (P("fs", None), P("fs", "tp"), P("fs", None), P("fs", "tp"), P("tp", "fs"))
    out_specs = (P("fs", None), P("fs", "tp"), P("tp", "fs"), P("fs"), P("tp"))
    return jax.shard_map(local, mesh=mesh, in_specs=in_specs, out_specs=out_specs, check_vma=False)
```

profile of v0, /device:TPU:0, one launch (start us, length us, event | category | flops | bytes accessed | tf_op | source)
XLA Modules:
  0.0 329.2 jit_solution(1895293256298894493)
XLA Ops:
  7.2 0.0 copy-start.2
  7.2 0.0 all-gather.5.cloned.1.call-start
  7.2 0.7 all-gather.5.cloned.1.call-update
  7.9 0.0 copy-start.1
  7.9 0.0 all-gather.11.cloned.1.call-start
  8.0 0.3 copy-done.2
  8.3 1.1 multiply_convert_fusion
  9.4 0.0 all-gather.11.cloned.1.call-update
  9.4 0.0 all-gather.7.cloned.1.call-start
  9.5 0.7 all-gather.7.cloned.1.call-update
  10.1 0.0 all-gather.9.cloned.1.call-start
  10.2 54.8 %all-gather.5.cloned.1.call-done = bf16[1024,2048]{1,0:T(8,128)(2,1)} async-done(((bf16[1024,512]{1,0:T(8,128)(2,1)}), bf16[1024,2048]{1,0:T(8,128)(2,1)}) %all-gather.5.cloned.1.call-update) | async-done | bytes 4194320 | tf_op jit(solution)/shard_map/all_gather | solution.py:22
  65.0 0.0 copy-done.1
  65.0 0.0 copy-start
  65.0 5.2 %multiply_convert_fusion.1 = bf16[384,1024]{1,0:T(8,128)(2,1)} fusion(bf16[384,1024]{1,0:T(8,128)(2,1)} %param.6, bf16[384,2048]{1,0:T(8,128)(2,1)S(1)} %copy-done.1, bf16[1024,2048]{1,0:T(8,128)(2,1)} %all-gather.5.cloned.1.call-done), kind=kOutput, calls=%fused_computation.4 | convolution fusion | flops 1612578816 | bytes 7340032 | tf_op jit(solution)/shard_map/dot_general | solution.py:8
  70.2 0.0 all-gather.9.cloned.1.call-update
  70.3 0.0 copy-done
  70.3 1.6 copy.14
  71.8 3.6 %all-to-all-start = ((bf16[384,4,512]{0,2,1:T(8,128)(2,1)}), bf16[384,4,512]{0,2,1:T(8,128)(2,1)S(1)}, u32[]{:S(2)}, u32[]{:S(2)}) async-start(bf16[384,4,512]{0,2,1:T(8,128)(2,1)} %bitcast), calls=%async_computation | async-start | bytes 3145728 | tf_op jit(solution)/shard_map/all_to_all | solution.py:27
  75.5 1.6 copy.16
  77.0 25.8 %all-to-all-done = bf16[384,4,512]{0,2,1:T(8,128)(2,1)S(1)} async-done(((bf16[384,4,512]{0,2,1:T(8,128)(2,1)}), bf16[384,4,512]{0,2,1:T(8,128)(2,1)S(1)}, u32[]{:S(2)}, u32[]{:S(2)}) %all-to-all-start) | async-done | bytes 1572896 | tf_op jit(solution)/shard_map/all_to_all | solution.py:27
  102.9 3.6 %all-to-all-start.1 = ((bf16[384,4,512]{0,2,1:T(8,128)(2,1)}), bf16[384,4,512]{0,2,1:T(8,128)(2,1)S(1)}, u32[]{:S(2)}, u32[]{:S(2)}) async-start(bf16[384,4,512]{0,2,1:T(8,128)(2,1)} %bitcast.4), calls=%async_computation.1 | async-start | bytes 3145728 | tf_op jit(solution)/shard_map/all_to_all | solution.py:28
  106.4 1.6 copy.15
  108.1 34.6 %all-to-all-done.1 = bf16[384,4,512]{0,2,1:T(8,128)(2,1)S(1)} async-done(((bf16[384,4,512]{0,2,1:T(8,128)(2,1)}), bf16[384,4,512]{0,2,1:T(8,128)(2,1)S(1)}, u32[]{:S(2)}, u32[]{:S(2)}) %all-to-all-start.1) | async-done | bytes 1572896 | tf_op jit(solution)/shard_map/all_to_all | solution.py:28
  142.7 1.6 copy.17
  144.3 0.0 all-gather.11.cloned.1.call-done
  144.3 4.2 %multiply_reduce_fusion = (f32[1024]{0:T(1024)S(1)}, f32[1024,512]{0,1:T(8,128)S(1)}) fusion(bf16[1536,1024]{1,0:T(8,128)(2,1)} %all-gather.11.cloned.1.call-done, bf16[1536,512]{1,0:T(8,128)(2,1)} %bitcast.19), kind=kOutput, calls=%fused_computation | convolution fusion | flops 1611660288 | bytes 6819840 | tf_op jit(solution)/shard_map/dot_general | solution.py:14
  148.5 1.8 copy.19
  150.3 9.8 %psum.23 = f32[1024]{0:T(1024)} all-reduce(f32[1024]{0:T(1024)S(1)} %get-tuple-element.24), channel_id=1, replica_groups=mesh['fs'=4,'tp'=8] {'fs'}, use_global_device_ids=true, to_apply=%region_4.0 | all-reduce | flops 1024 | bytes 8192 | tf_op jit(solution)/shard_map/psum | solution.py:37
  160.1 37.4 %all-gather.7.cloned.1.call-done = bf16[2048,1024]{1,0:T(8,128)(2,1)} async-done(((bf16[512,1024]{1,0:T(8,128)(2,1)}), bf16[2048,1024]{1,0:T(8,128)(2,1)}) %all-gather.7.cloned.1.call-update) | async-done | bytes 4194320 | tf_op jit(solution)/shard_map/all_gather | solution.py:24
  197.5 4.3 %fusion = f32[384,2048]{1,0:T(8,128)S(1)} fusion(bf16[384,1024]{1,0:T(8,128)(2,1)} %multiply_convert_fusion.1, bf16[2048,1024]{1,0:T(8,128)(2,1)} %all-gather.7.cloned.1.call-done), kind=kOutput, calls=%fused_computation.6 | convolution fusion | flops 1610612736 | bytes 8126464 | tf_op jit(solution)/shard_map/dot_general | solution.py:8
  201.7 41.9 %all-gather.9.cloned.1.call-done = bf16[1536,1024]{1,0:T(8,128)(2,1)} async-done(((bf16[384,1024]{1,0:T(8,128)(2,1)}), bf16[1536,1024]{1,0:T(8,128)(2,1)}) %all-gather.9.cloned.1.call-update) | async-done | bytes 3145744 | tf_op jit(solution)/shard_map/all_gather | solution.py:31
  243.6 5.5 %multiply_reduce_fusion.1 = (f32[512]{0:T(512)S(1)}, f32[512,1024]{0,1:T(8,128)}) fusion(bf16[1536,1024]{1,0:T(8,128)(2,1)} %all-gather.9.cloned.1.call-done, bf16[1536,512]{1,0:T(8,128)(2,1)} %bitcast.18), kind=kOutput, calls=%fused_computation.1 | convolution fusion | flops 1611660800 | bytes 6817792 | tf_op jit(solution)/shard_map/dot_general | solution.py:14
  249.1 2.9 copy.18
  252.0 70.7 %all-reduce.2 = (bf16[384,2048]{1,0:T(8,128)(2,1)}, f32[512]{0:T(512)}) all-reduce(f32[384,2048]{1,0:T(8,128)S(1)} %fusion, f32[512]{0:T(512)S(1)} %get-tuple-element.22), channel_id=1, replica_groups=mesh['fs'=4,'tp'=8] {'tp'}, use_global_device_ids=true, to_apply=%region_0.0 | all-reduce | flops 786944 | bytes 4722688 | tf_op jit(solution)/shard_map/psum | solution.py:25
Async XLA Ops:
  7.2 1.1 copy-start.2
  7.2 57.8 %all-gather.5.cloned.1.call-start = ((), (), s32[]{:S(2)}) async-start(), calls=%async_computation.2 | async-start | bytes 5242880 | tf_op jit(solution)/shard_map/all_gather | solution.py:22
  7.9 57.1 %copy-start.1 = (bf16[384,2048]{1,0:T(8,128)(2,1)S(1)}, bf16[384,2048]{1,0:T(8,128)(2,1)}, u32[]{:S(2)}) copy-start(bf16[384,2048]{1,0:T(8,128)(2,1)} %param.7) | copy-start | bytes 4718596
  7.9 136.4 %all-gather.11.cloned.1.call-start = ((), (), s32[]{:S(2)}) async-start(), calls=%async_computation.5 | async-start | bytes 3932160 | tf_op jit(solution)/shard_map/all_gather | solution.py:32
  9.4 188.1 %all-gather.7.cloned.1.call-start = ((), (), s32[]{:S(2)}) async-start(), calls=%async_computation.3 | async-start | bytes 5242880 | tf_op jit(solution)/shard_map/all_gather | solution.py:24
  10.1 233.5 %all-gather.9.cloned.1.call-start = ((), (), s32[]{:S(2)}) async-start(), calls=%async_computation.4 | async-start | bytes 3932160 | tf_op jit(solution)/shard_map/all_gather | solution.py:31
  65.0 5.3 %copy-start = (bf16[384,2048]{1,0:T(8,128)(2,1)S(1)}, bf16[384,2048]{1,0:T(8,128)(2,1)}, u32[]{:S(2)}) copy-start(bf16[384,2048]{1,0:T(8,128)(2,1)} %param.5) | copy-start | bytes 4718596
  71.8 31.0 %all-to-all-start = ((bf16[384,4,512]{0,2,1:T(8,128)(2,1)}), bf16[384,4,512]{0,2,1:T(8,128)(2,1)S(1)}, u32[]{:S(2)}, u32[]{:S(2)}) async-start(bf16[384,4,512]{0,2,1:T(8,128)(2,1)} %bitcast), calls=%async_computation | async-start | bytes 3145728 | tf_op jit(solution)/shard_map/all_to_all | solution.py:27
  102.9 39.8 %all-to-all-start.1 = ((bf16[384,4,512]{0,2,1:T(8,128)(2,1)}), bf16[384,4,512]{0,2,1:T(8,128)(2,1)S(1)}, u32[]{:S(2)}, u32[]{:S(2)}) async-start(bf16[384,4,512]{0,2,1:T(8,128)(2,1)} %bitcast.4), calls=%async_computation.1 | async-start | bytes 3145728 | tf_op jit(solution)/shard_map/all_to_all | solution.py:28
Sparse Core Ops, SparseCore 0:
  9.8 55.1 all-gather.4
  66.8 76.1 all-gather.10
  144.8 52.5 all-gather.6
  199.8 43.8 all-gather.8
where the time goes:
time: 330 us; the launch traced here: 329 us
  waiting for transfers between devices  196 us (59%)
  blocking collectives  80.5 us (24%)
  matrix products  19.2 us (6%)
  between operations  13.8 us (4%)
  local copies, waits for them, and re-layouts  11.4 us (3%)
  starting transfers between devices  7.33 us (2%)
    psum x1, blocking collectives, local(): input_grad = lax.psum(partial_value, 'tp').astype(jnp.bfloat16)  70.7 us
    all_gather x1, waiting for transfers between devices, local(): lax.all_gather(down_weight, 'fs', axis=1, tiled=True)  54.8 us
    all_gather x1, waiting for transfers between devices, local(): lax.all_gather(pre_grad, 'fs', axis=0, tiled=True)  41.9 us
    all_gather x1, waiting for transfers between devices, local(): lax.all_gather(up_weight, 'fs', axis=0, tiled=True)  37.4 us
    all_to_all x1, waiting for transfers between devices, local(): lax.all_to_all(cotangent, 'fs', split_axis=1, concat_axis=0, tiled=True)  34.6 us
    all_to_all x1, waiting for transfers between devices, local(): lax.all_to_all(inputs, 'fs', split_axis=1, concat_axis=0, tiled=True)  25.8 us
    psum x1, blocking collectives, local(): down_norms = lax.psum(jnp.sum(down_grad * down_grad, axis=1), 'fs')  9.78 us
    dot_general x2, matrix products, contract_first(): lax.dot_general(left, right, (((0,), (0,)), ((), ())), preferred_element_...  9.7 us
  transfers between devices with their start and end apart: 6, of which 5 were waited for; matrix products, arithmetic and copies ran while one was open for 7% of the time, Pallas kernels for 0%

commit v1 on v0

--- a/solution.py
+++ b/solution.py
@@ -22,7 +22,7 @@
     sq_grad = contract_last(cotangent, lax.all_gather(down_weight, "fs", axis=1, tiled=True))
     pre_grad = (2.0 * active * sq_grad).astype(jnp.bfloat16)
     partial_value = contract_last(pre_grad, lax.all_gather(up_weight, "fs", axis=0, tiled=True))
-    input_grad = lax.psum(partial_value, "tp").astype(jnp.bfloat16)
+    input_grad = jnp.sum(lax.all_gather(partial_value, "tp"), axis=0).astype(jnp.bfloat16)
     input_cols, cotan_cols = (
         lax.all_to_all(inputs, "fs", split_axis=1, concat_axis=0, tiled=True),
         lax.all_to_all(cotangent, "fs", split_axis=1, concat_axis=0, tiled=True),

time: 330 us -> 480 us (1.45)
  waiting for transfers between devices: 196 us -> 389 us
  blocking collectives: 80.5 us -> 27.3 us
  other arithmetic: 1.08 us -> 11.8 us
    all_gather x0 -> x1, waiting for transfers between devices: none -> 198 us  [local(): lax.all_gather(partial_value, 'tp')]
    psum x1, blocking collectives: 70.7 us -> 17.4 us  [local(): up_norms = lax.psum(jnp.sum(up_grad * up_grad, axis=1), 'tp')]
    all_gather x1, waiting for transfers between devices: 41.9 us -> 28 us  [local(): lax.all_gather(pre_grad, 'fs', axis=0, tiled=True)]
    all_gather x1, waiting for transfers between devices: 37.4 us -> 49.5 us  [local(): lax.all_gather(up_weight, 'fs', axis=0, tiled=True)]
    reduce_sum x0 -> x1, other arithmetic: none -> 10.7 us  [local(): jnp.sum(lax.all_gather(partial_value, 'tp'), axis=0).astype(jnp.bfloat16)]
  transfers between devices with their start and end apart: 6 -> 7, of which waited for: 5 -> 6; matrix products, arithmetic and copies ran while one was open for 7% -> 6% of each run, Pallas kernels for 0% -> 0%
where the time goes in v1:
time: 480 us
  waiting for transfers between devices  389 us (81%)
  blocking collectives  27.3 us (6%)
  matrix products  19.2 us (4%)
  between operations  13.8 us (3%)
  other arithmetic  11.8 us (2%)
  local copies, waits for them, and re-layouts  11.4 us (2%)
  starting transfers between devices  7.44 us (2%)
    all_gather x1, waiting for transfers between devices, local(): lax.all_gather(partial_value, 'tp')  198 us
    all_gather x1, waiting for transfers between devices, local(): lax.all_gather(down_weight, 'fs', axis=1, tiled=True)  55.1 us
    all_gather x1, waiting for transfers between devices, local(): lax.all_gather(up_weight, 'fs', axis=0, tiled=True)  49.5 us
    all_to_all x1, waiting for transfers between devices, local(): lax.all_to_all(cotangent, 'fs', split_axis=1, concat_axis=0, tiled=True)  32.9 us
    all_gather x1, waiting for transfers between devices, local(): lax.all_gather(pre_grad, 'fs', axis=0, tiled=True)  28 us
    all_to_all x1, waiting for transfers between devices, local(): lax.all_to_all(inputs, 'fs', split_axis=1, concat_axis=0, tiled=True)  23.9 us
    psum x1, blocking collectives, local(): up_norms = lax.psum(jnp.sum(up_grad * up_grad, axis=1), 'tp')  17.4 us
    dot_general x2, matrix products, contract_last(): lax.dot_general(left, right, (((1,), (1,)), ((), ())), preferred_element_...  10.8 us
  transfers between devices with their start and end apart: 7, of which 6 were waited for; matrix products, arithmetic and copies ran while one was open for 6% of the time, Pallas kernels for 0%

profile of v1, /device:TPU:0, one launch (start us, length us, event | category | flops | bytes accessed | tf_op | source)
XLA Modules:
  0.0 479.8 jit_solution(7824727163421122589)
XLA Ops:
  7.2 0.0 copy-start.2
  7.2 0.0 all-gather.7.cloned.1.call-start
  7.2 0.7 all-gather.7.cloned.1.call-update
  7.9 0.0 copy-start.1
  7.9 0.0 all-gather.9.cloned.1.call-start
  8.0 0.7 all-gather.9.cloned.1.call-update
  8.7 0.0 all-gather.13.cloned.1.call-start
  8.7 0.0 copy-done.2
  8.7 1.1 multiply_convert_fusion
  9.8 0.0 all-gather.13.cloned.1.call-update
  9.9 0.0 all-gather.11.cloned.1.call-start
  9.9 55.1 %all-gather.7.cloned.1.call-done = bf16[1024,2048]{1,0:T(8,128)(2,1)} async-done(((bf16[1024,512]{1,0:T(8,128)(2,1)}), bf16[1024,2048]{1,0:T(8,128)(2,1)}) %all-gather.7.cloned.1.call-update) | async-done | bytes 4194320 | tf_op jit(solution)/shard_map/all_gather | solution.py:22
  65.0 0.0 copy-done.1
  65.0 4.9 %multiply_convert_fusion.1 = bf16[384,1024]{1,0:T(8,128)(2,1)} fusion(bf16[384,1024]{1,0:T(8,128)(2,1)S(1)} %copy-done.2, bf16[384,2048]{1,0:T(8,128)(2,1)S(1)} %copy-done.1, bf16[1024,2048]{1,0:T(8,128)(2,1)} %all-gather.7.cloned.1.call-done), kind=kOutput, calls=%fused_computation.4 | convolution fusion | flops 1612578816 | bytes 7340032 | tf_op jit(solution)/shard_map/dot_general | solution.py:8
  69.9 0.0 all-gather.11.cloned.1.call-update
  69.9 0.0 all-gather.15.cloned.1.call-start
  70.0 49.5 %all-gather.9.cloned.1.call-done = bf16[2048,1024]{1,0:T(8,128)(2,1)} async-done(((bf16[512,1024]{1,0:T(8,128)(2,1)}), bf16[2048,1024]{1,0:T(8,128)(2,1)}) %all-gather.9.cloned.1.call-update) | async-done | bytes 4194320 | tf_op jit(solution)/shard_map/all_gather | solution.py:24
  119.5 5.9 %fusion = f32[384,2048]{1,0:T(8,128)} fusion(bf16[384,1024]{1,0:T(8,128)(2,1)} %multiply_convert_fusion.1, bf16[2048,1024]{1,0:T(8,128)(2,1)} %all-gather.9.cloned.1.call-done), kind=kOutput, calls=%fused_computation.6 | convolution fusion | flops 1610612736 | bytes 8126464 | tf_op jit(solution)/shard_map/dot_general | solution.py:8
  125.3 0.0 copy-start
  125.3 0.0 all-gather.15.cloned.1.call-update
  125.4 1.4 copy-done
  126.7 1.6 copy.14
  128.3 3.6 all-to-all-start
  131.9 1.6 copy.16
  133.4 23.9 %all-to-all-done = bf16[384,4,512]{0,2,1:T(8,128)(2,1)S(1)} async-done(((bf16[384,4,512]{0,2,1:T(8,128)(2,1)}), bf16[384,4,512]{0,2,1:T(8,128)(2,1)S(1)}, u32[]{:S(2)}, u32[]{:S(2)}) %all-to-all-start) | async-done | bytes 1572896 | tf_op jit(solution)/shard_map/all_to_all | solution.py:27
  157.3 3.7 all-to-all-start.1
  161.0 1.6 copy.15
  162.6 32.9 %all-to-all-done.1 = bf16[384,4,512]{0,2,1:T(8,128)(2,1)S(1)} async-done(((bf16[384,4,512]{0,2,1:T(8,128)(2,1)}), bf16[384,4,512]{0,2,1:T(8,128)(2,1)S(1)}, u32[]{:S(2)}, u32[]{:S(2)}) %all-to-all-start.1) | async-done | bytes 1572896 | tf_op jit(solution)/shard_map/all_to_all | solution.py:28
  195.5 1.6 copy.17
  197.1 0.0 all-gather.13.cloned.1.call-done
  197.1 4.2 multiply_reduce_fusion
  201.3 1.8 copy.19
  203.1 10.0 %psum.15 = f32[1024]{0:T(1024)} all-reduce(f32[1024]{0:T(1024)S(1)} %get-tuple-element.22), channel_id=1, replica_groups=mesh['fs'=4,'tp'=8] {'fs'}, use_global_device_ids=true, to_apply=%region_4.0 | all-reduce | flops 1024 | bytes 8192 | tf_op jit(solution)/shard_map/psum | solution.py:37
  213.1 28.0 %all-gather.11.cloned.1.call-done = bf16[1536,1024]{1,0:T(8,128)(2,1)} async-done(((bf16[384,1024]{1,0:T(8,128)(2,1)}), bf16[1536,1024]{1,0:T(8,128)(2,1)}) %all-gather.11.cloned.1.call-update) | async-done | bytes 3145744 | tf_op jit(solution)/shard_map/all_gather | solution.py:31
  241.1 4.2 multiply_reduce_fusion.1
  245.3 1.8 copy.18
  247.1 17.4 %psum.14 = f32[512]{0:T(512)} all-reduce(f32[512]{0:T(512)S(1)} %get-tuple-element.20), channel_id=1, replica_groups=mesh['fs'=4,'tp'=8] {'tp'}, use_global_device_ids=true, to_apply=%region_2.0 | all-reduce | flops 512 | bytes 4096 | tf_op jit(solution)/shard_map/psum | solution.py:36
  264.5 198.1 %all-gather.15.cloned.1.call-done = f32[3072,2048]{1,0:T(8,128)} async-done(((f32[384,2048]{1,0:T(8,128)}), f32[3072,2048]{1,0:T(8,128)}) %all-gather.15.cloned.1.call-update) | async-done | bytes 25165840 | tf_op jit(solution)/shard_map/all_gather | solution.py:25
  462.6 10.7 %reduce_sum.27 = bf16[384,2048]{1,0:T(8,128)(2,1)} reduce(f32[8,384,2048]{2,1,0:T(8,128)} %bitcast.17, f32[]{:T(128)} %constant.2.clone.1), dimensions={0}, to_apply=%region_0.0 | reduce | flops 5505024 | bytes 26738692 | tf_op jit(solution)/shard_map/reduce_sum | solution.py:25
Async XLA Ops:
  7.2 1.6 copy-start.2
  7.2 57.8 %all-gather.7.cloned.1.call-start = ((), (), s32[]{:S(2)}) async-start(), calls=%async_computation.2 | async-start | bytes 5242880 | tf_op jit(solution)/shard_map/all_gather | solution.py:22
  7.9 57.1 %copy-start.1 = (bf16[384,2048]{1,0:T(8,128)(2,1)S(1)}, bf16[384,2048]{1,0:T(8,128)(2,1)}, u32[]{:S(2)}) copy-start(bf16[384,2048]{1,0:T(8,128)(2,1)} %param.7) | copy-start | bytes 4718596
  7.9 111.5 %all-gather.9.cloned.1.call-start = ((), (), s32[]{:S(2)}) async-start(), calls=%async_computation.3 | async-start | bytes 5242880 | tf_op jit(solution)/shard_map/all_gather | solution.py:24
  8.7 188.5 %all-gather.13.cloned.1.call-start = ((), (), s32[]{:S(2)}) async-start(), calls=%async_computation.5 | async-start | bytes 3932160 | tf_op jit(solution)/shard_map/all_gather | solution.py:32
  9.9 231.2 %all-gather.11.cloned.1.call-start = ((), (), s32[]{:S(2)}) async-start(), calls=%async_computation.4 | async-start | bytes 3932160 | tf_op jit(solution)/shard_map/all_gather | solution.py:31
  69.9 392.6 %all-gather.15.cloned.1.call-start = ((), (), s32[]{:S(2)}) async-start(), calls=%async_computation.6 | async-start | bytes 28311552 | tf_op jit(solution)/shard_map/all_gather | solution.py:25
  125.3 1.4 copy-start
  128.3 29.0 %all-to-all-start = ((bf16[384,4,512]{0,2,1:T(8,128)(2,1)}), bf16[384,4,512]{0,2,1:T(8,128)(2,1)S(1)}, u32[]{:S(2)}, u32[]{:S(2)}) async-start(bf16[384,4,512]{0,2,1:T(8,128)(2,1)} %bitcast.1), calls=%async_computation | async-start | bytes 3145728 | tf_op jit(solution)/shard_map/all_to_all | solution.py:27
  157.3 38.2 %all-to-all-start.1 = ((bf16[384,4,512]{0,2,1:T(8,128)(2,1)}), bf16[384,4,512]{0,2,1:T(8,128)(2,1)S(1)}, u32[]{:S(2)}, u32[]{:S(2)}) async-start(bf16[384,4,512]{0,2,1:T(8,128)(2,1)} %bitcast.5), calls=%async_computation.1 | async-start | bytes 3145728 | tf_op jit(solution)/shard_map/all_to_all | solution.py:28
Sparse Core Ops, SparseCore 0:
  9.8 55.1 all-gather.6
  66.8 52.5 all-gather.8
  121.3 74.4 all-gather.12
  198.1 42.9 all-gather.10
  242.6 219.9 all-gather.14
